TPU v7x, 32 devices: a whole 2x2x4 slice. The times are simulated.
32 devices in a mesh: rep: 2 (over x), fs: 4 (over z), tp: 4 (over y, core).
Axes of the slice: x: 2, y: 2, z: 4, core: 2. Of those that a mesh axis runs over, the one named last changes fastest.
Arguments:
- tokens: bfloat16 [8, 1024, 2048], P(('rep', 'fs')), may hold values from -6 to 6
- mix_gain: bfloat16 [2048], replicated, may hold values from 0.099609375 to 1.8984375
- value_weight: bfloat16 [2048, 1024], P('fs', 'tp'), may hold values from -0.125 to 0.125
- gate_weight: bfloat16 [2048, 1024], P('fs', 'tp'), may hold values from -0.125 to 0.125
- mix_taps: bfloat16 [31, 1024], P(None, 'tp'), may hold values from -1 to 1
- head_gain: bfloat16 [1024], P('tp'), may hold values from 0.099609375 to 1.8984375
- out_weight: bfloat16 [1024, 2048], P('fs', 'tp'), may hold values from -0.1875 to 0.1875
- ffn_gain: bfloat16 [2048], replicated, may hold values from 0.099609375 to 1.8984375
- ffgate_weight: bfloat16 [2048, 6144], P('fs', 'tp'), may hold values from -0.125 to 0.125
- up_weight: bfloat16 [2048, 6144], P('fs', 'tp'), may hold values from -0.125 to 0.125
- ff_taps: bfloat16 [3, 6144], P(None, 'tp'), may hold values from -3.5 to 3.5
- down_weight: bfloat16 [2048, 6144], P('fs', 'tp'), may hold values from -0.078125 to 0.078125
Outputs:
- layer_out: bfloat16 [8, 1024, 2048], P(('rep', 'fs'), 'tp')
All inputs are finite; a program needn't handle non-finite values.
Results may differ from a plain program's by a relative error of at most 0.01.
Values may be sent and summed in bfloat16 or wider, within the bound.
No kernel may reach another device: no remote copies, remote signals or barrier semaphores. Data moves between devices by JAX's collectives and lax.ppermute only.
A program may use at most 128 MiB of HBM per device.

v0:
```python
import jax
import jax.numpy as jnp
from jax import lax
from jax.sharding import PartitionSpec as P

HEAD = 128
norm_floor = 0.01


def row_norm(floats_in, scales):
    floats = floats_in.astype(jnp.float32)
    scaled = floats * lax.rsqrt(jnp.mean(floats * floats, axis=-1, keepdims=True) + norm_floor)
    return (scaled * scales.astype(jnp.float32)).astype(jnp.bfloat16)


def causal_conv(signal, kernel_taps):
    reach = kernel_taps.shape[0]
    length = signal.shape[0]
    padded = jnp.pad(signal, ((reach - 1, 0), (0, 0)))
    summed = padded[0:length] * kernel_taps[0]
    for offset in range(1, reach):
        summed = summed + padded[offset : offset + length] * kernel_taps[offset]
    return summed


def head_norm(signal, scales):
    length = signal.shape[0]
    grouped = signal.reshape(length, signal.shape[1] // HEAD, HEAD)
    centre = grouped - jnp.mean(grouped, axis=-1, keepdims=True)
    spread = jnp.mean(centre * centre, axis=-1, keepdims=True)
    normal = (centre * lax.rsqrt(spread + norm_floor)).reshape(signal.shape)
    return normal * scales.astype(jnp.float32)


def on_device(
    tokens,
    mix_gain,
    value_weight,
    gate_weight,
    mix_taps,
    head_gain,
    out_weight,
    ffn_gain,
    ffgate_weight,
    up_weight,
    ff_taps,
    down_weight,
):
    sequence = tokens[0]
    value_full, gate_full, out_full = (
        lax.all_gather(value_weight, "fs", axis=0, tiled=True),
        lax.all_gather(gate_weight, "fs", axis=0, tiled=True),
        lax.all_gather(out_weight, "fs", axis=0, tiled=True),
    )
    normed = row_norm(sequence, mix_gain)
    values = jnp.dot(normed, value_full, preferred_element_type=jnp.float32)
    gating = jnp.dot(normed, gate_full, preferred_element_type=jnp.float32)
    glu_out = values * jax.nn.sigmoid(gating)
    mixed_pos = causal_conv(glu_out, mix_taps.astype(jnp.float32))
    head_out = jax.nn.silu(head_norm(mixed_pos, head_gain)).astype(jnp.bfloat16)
    out_cols = out_full.shape[1]
    mixer_sum = jnp.dot(
        lax.all_gather(head_out, "tp", axis=1, tiled=True),
        out_full,
        preferred_element_type=jnp.float32,
    )
    own_cols = lax.dynamic_slice_in_dim(sequence, lax.axis_index("tp") * out_cols, out_cols, 1)
    hidden_cols = (own_cols.astype(jnp.float32) + mixer_sum).astype(jnp.bfloat16)
    full_rows = lax.all_gather(hidden_cols, "tp", axis=1, tiled=True)
    normed_ffn = row_norm(full_rows, ffn_gain)
    block_rows = normed_ffn
    ffgate = jnp.dot(
        block_rows,
        lax.all_gather(ffgate_weight, "fs", axis=0, tiled=True),
        preferred_element_type=jnp.float32,
    )
    ff_up = jnp.dot(
        block_rows,
        lax.all_gather(up_weight, "fs", axis=0, tiled=True),
        preferred_element_type=jnp.float32,
    )
    down_full = lax.all_gather(down_weight, "fs", axis=0, tiled=True)
    product = (jax.nn.silu(causal_conv(ffgate, ff_taps.astype(jnp.float32))) * ff_up).astype(
        jnp.bfloat16
    )
    own_count = sequence.shape[0] // lax.axis_size("tp")
    block_rows = product
    summed_rows = lax.psum_scatter(
        lax.dot_general(
            block_rows, down_full, (((1,), (1,)), ((), ())), preferred_element_type=jnp.float32
        ).astype(jnp.bfloat16),
        "tp",
        scatter_dimension=0,
        tiled=True,
    ).astype(jnp.float32)
    own_rows = lax.dynamic_slice_in_dim(full_rows, lax.axis_index("tp") * own_count, own_count, 0)
    return (own_rows.astype(jnp.float32) + summed_rows).astype(jnp.bfloat16)[None]


def solution(mesh):
    placed = (
        P(("rep", "fs"), None, None),
        P(),
        P("fs", "tp"),
        P("fs", "tp"),
        P(None, "tp"),
        P("tp"),
        P("fs", "tp"),
        P(),
        P("fs", "tp"),
        P("fs", "tp"),
        P(None, "tp"),
        P("fs", "tp"),
    )
    return jax.shard_map(
        on_device,
        mesh=mesh,
        in_specs=placed,
        out_specs=P(("rep", "fs"), "tp", None),
        check_vma=False,
    )
```

profile of v0, /device:TPU:0, one launch (start us, length us, event | category | flops | bytes accessed | tf_op | source)
XLA Modules:
  0.0 585.6 jit_solution(9061015034751386322)
XLA Ops:
  6.5 0.7 all-gather.11.cloned.1.call-update
  7.3 0.0 all-gather.9.cloned.1.call-start
  7.3 0.7 all-gather.9.cloned.1.call-update
  8.0 0.0 all-gather.15.cloned.1.call-start
  8.1 0.7 all-gather.15.cloned.1.call-update
  8.7 0.0 all-gather.13.cloned.1.call-start
  8.8 1.0 fusion.38
  9.8 1.0 fusion.39
  10.8 3.1 fusion.3
  13.9 0.7 convert_element_type.65
  14.6 0.7 convert_element_type.68
  15.2 24.4 %all-gather.11.cloned.1.call-done = bf16[2048,256]{1,0:T(8,128)(2,1)} async-done(((bf16[512,256]{1,0:T(8,128)(2,1)}), bf16[2048,256]{1,0:T(8,128)(2,1)}) %all-gather.11.cloned.1.call-update) | async-done | bytes 1048592 | tf_op jit(solution)/shard_map/all_gather | solution.py:52
  39.6 3.8 fusion.9
  43.5 25.1 %all-gather.9.cloned.1.call-done = bf16[2048,256]{1,0:T(8,128)(2,1)} async-done(((bf16[512,256]{1,0:T(8,128)(2,1)}), bf16[2048,256]{1,0:T(8,128)(2,1)}) %all-gather.9.cloned.1.call-update) | async-done | bytes 1048592 | tf_op jit(solution)/shard_map/all_gather | solution.py:51
  68.6 3.8 convolution_multiply_fusion
  72.4 4.2 multiply_add_fusion
  76.6 0.5 reshape.42
  77.2 1.1 reduce_sum.37
  78.4 14.4 %multiply_reduce_fusion = f32[1024,2]{1,0:T(8,128)S(1)} fusion(f32[1024,2,128]{2,1,0:T(2,128)S(1)} %reshape.42, f32[1024,2]{1,0:T(8,128)S(1)} %broadcast_multiply_fusion), kind=kLoop, calls=%fused_computation.26 | loop fusion | flops 784384 | bytes 1064960 | tf_op jit(solution)/shard_map/reduce_sum | solution.py:30
  92.8 0.1 add_rsqrt_fusion
  92.9 1.2 mul.521
  94.1 1.2 sub.13
  95.4 5.8 multiply_convert_fusion.1
  101.2 0.0 all-gather.13.cloned.1.call-update
  101.2 0.0 all-gather.17.cloned.1.call-start
  101.2 0.0 copy-start.1
  101.3 0.0 all-gather.15.cloned.1.call-done
  101.3 22.2 %all-gather.13.cloned.1.call-done = bf16[1024,1024]{1,0:T(8,128)(2,1)} async-done(((bf16[1024,256]{1,0:T(8,128)(2,1)}), bf16[1024,1024]{1,0:T(8,128)(2,1)}) %all-gather.13.cloned.1.call-update) | async-done | bytes 2097168 | tf_op jit(solution)/shard_map/all_gather | solution.py:63
  123.5 4.4 fusion.6
  127.9 0.0 all-gather.17.cloned.1.call-update
  128.0 0.0 all-gather.19.cloned.1.call-start
  128.0 0.5 all-gather.19.cloned.1.call-update
  128.5 0.0 all-gather.21.cloned.1.call-start
  128.6 0.7 all-gather.21.cloned.1.call-update
  129.3 0.0 all-gather.23.cloned.1.call-start
  129.3 0.7 all-gather.23.cloned.1.call-update
  130.0 0.0 reduce-scatter.2.cloned.1.call-start
  130.1 0.1 slice_reduce_fusion.2
  130.2 32.4 %all-gather.17.cloned.1.call-done = bf16[1024,2048]{1,0:T(8,128)(2,1)} async-done(((bf16[1024,512]{1,0:T(8,128)(2,1)}), bf16[1024,2048]{1,0:T(8,128)(2,1)}) %all-gather.17.cloned.1.call-update) | async-done | bytes 4194320 | tf_op jit(solution)/shard_map/all_gather | solution.py:69
  162.6 3.1 fusion
  165.7 113.7 %all-gather.19.cloned.1.call-done = bf16[2048,1536]{1,0:T(8,128)(2,1)} async-done(((bf16[512,1536]{1,0:T(8,128)(2,1)}), bf16[2048,1536]{1,0:T(8,128)(2,1)}) %all-gather.19.cloned.1.call-update) | async-done | bytes 6291472 | tf_op jit(solution)/shard_map/all_gather | solution.py:74
  279.4 12.2 %fusion.11 = f32[1024,1536]{1,0:T(8,128)} fusion(bf16[2048,1536]{1,0:T(8,128)(2,1)} %all-gather.19.cloned.1.call-done, bf16[1024,2048]{1,0:T(8,128)(2,1)} %all-gather.17.cloned.1.call-done, f32[2048]{0:T(1024)S(1)} %convert_element_type.73, f32[1024]{0:T(1024)S(1)} %add_rsqrt_fusion.1), kind=kOutput, calls=%fused_computation.20 | convolution fusion | flops 6450839552 | bytes 16789504 | tf_op jit(solution)/shard_map/dot_general | solution.py:72
  291.5 102.9 %all-gather.21.cloned.1.call-done = bf16[2048,1536]{1,0:T(8,128)(2,1)} async-done(((bf16[512,1536]{1,0:T(8,128)(2,1)}), bf16[2048,1536]{1,0:T(8,128)(2,1)}) %all-gather.21.cloned.1.call-update) | async-done | bytes 6291472 | tf_op jit(solution)/shard_map/all_gather | solution.py:79
  394.5 115.1 %all-gather.23.cloned.1.call-done = bf16[2048,1536]{1,0:T(8,128)(2,1)} async-done(((bf16[512,1536]{1,0:T(8,128)(2,1)}), bf16[2048,1536]{1,0:T(8,128)(2,1)}) %all-gather.23.cloned.1.call-update) | async-done | bytes 6291472 | tf_op jit(solution)/shard_map/all_gather | solution.py:82
  509.6 23.6 %convolution_convert_fusion = bf16[1024,2048]{1,0:T(8,128)(2,1)} fusion(bf16[2048,1536]{1,0:T(8,128)(2,1)} %all-gather.23.cloned.1.call-done, f32[1024,1536]{1,0:T(8,128)} %fusion.11, bf16[2048,1536]{1,0:T(8,128)(2,1)} %all-gather.21.cloned.1.call-done, f32[1536]{0:T(1024)S(1)} %get-tuple-element.6, f32[1536]{0:T(1024)S(1)} %get-tuple-element.7, ...), kind=kOutput, calls=%fused_computation.11 | convolution fusion | flops 12912689152 | bytes 27293696 | tf_op jit(solution)/shard_map/dot_general | solution.py:89
  533.2 0.0 reduce-scatter.2.cloned.1.call-update
  533.2 42.9 %reduce-scatter.2.cloned.1.call-done = bf16[256,2048]{1,0:T(8,128)(2,1)} async-done(((bf16[1024,2048]{1,0:T(8,128)(2,1)}), bf16[256,2048]{1,0:T(8,128)(2,1)}) %reduce-scatter.2.cloned.1.call-update) | async-done | bytes 1048592 | tf_op jit(solution)/shard_map/reduce_scatter | solution.py:88
  576.1 2.9 fusion.15
  (9 shorter events, 0.1 us)
Async XLA Ops:
  6.5 33.1 %all-gather.11.cloned.1.call-start = ((), (), s32[]{:S(2)}) async-start(), calls=%async_computation.2 | async-start | bytes 1310720 | tf_op jit(solution)/shard_map/all_gather | solution.py:52
  7.3 61.3 %all-gather.9.cloned.1.call-start = ((), (), s32[]{:S(2)}) async-start(), calls=%async_computation.1 | async-start | bytes 1310720 | tf_op jit(solution)/shard_map/all_gather | solution.py:51
  8.0 93.3 %all-gather.15.cloned.1.call-start = ((), (), s32[]{:S(2)}) async-start(), calls=%async_computation.4 | async-start | bytes 1310720 | tf_op jit(solution)/shard_map/all_gather | solution.py:53
  8.7 114.8 %all-gather.13.cloned.1.call-start = ((), (), s32[]{:S(2)}) async-start(), calls=%async_computation.3 | async-start | bytes 2621440 | tf_op jit(solution)/shard_map/all_gather | solution.py:63
  101.2 61.4 %all-gather.17.cloned.1.call-start = ((), (), s32[]{:S(2)}) async-start(), calls=%async_computation.5 | async-start | bytes 5242880 | tf_op jit(solution)/shard_map/all_gather | solution.py:69
  101.2 28.8 %copy-start.1 = (bf16[2048]{0:T(1024)(128)(2,1)S(1)}, bf16[2048]{0:T(1024)(128)(2,1)}, u32[]{:S(2)}) copy-start(bf16[2048]{0:T(1024)(128)(2,1)} %param.19) | copy-start | bytes 12292
  101.3 28.9 %copy-start = (bf16[3,1536]{1,0:T(4,128)(2,1)S(1)}, bf16[3,1536]{1,0:T(4,128)(2,1)}, u32[]{:S(2)}) copy-start(bf16[3,1536]{1,0:T(4,128)(2,1)} %param.22) | copy-start | bytes 27652
  128.0 151.4 %all-gather.19.cloned.1.call-start = ((), (), s32[]{:S(2)}) async-start(), calls=%async_computation.6 | async-start | bytes 7864320 | tf_op jit(solution)/shard_map/all_gather | solution.py:74
  128.5 265.9 %all-gather.21.cloned.1.call-start = ((), (), s32[]{:S(2)}) async-start(), calls=%async_computation.7 | async-start | bytes 7864320 | tf_op jit(solution)/shard_map/all_gather | solution.py:79
  129.3 380.3 %all-gather.23.cloned.1.call-start = ((), (), s32[]{:S(2)}) async-start(), calls=%async_computation.8 | async-start | bytes 7864320 | tf_op jit(solution)/shard_map/all_gather | solution.py:82
  130.0 446.1 %reduce-scatter.2.cloned.1.call-start = ((), (), s32[]{:S(2)}) async-start(), calls=%async_computation.9 | async-start | bytes 5242880 | tf_op jit(solution)/shard_map/reduce_scatter | solution.py:88
Sparse Core Ops, SparseCore 0:
  8.9 30.6 all-gather.10
  41.2 27.3 all-gather.8
  70.2 27.3 all-gather.14
  101.3 22.1 all-gather.12
  128.1 34.4 all-gather.16
  164.0 115.3 all-gather.18
  280.9 113.4 all-gather.20
  396.0 113.5 all-gather.22
  533.3 42.7 reduce-scatter.1
where the time goes:
time: 586 us
  waiting for transfers between devices  483 us (82%)
  matrix products  47.8 us (8%)
  other arithmetic  36.1 us (6%)
  between operations  13.4 us (2%)
    all_gather x1, waiting for transfers between devices, on_device(): down_full = lax.all_gather(down_weight, 'fs', axis=0, tiled=True)  115 us
    all_gather x1, waiting for transfers between devices, on_device(): lax.all_gather(ffgate_weight, 'fs', axis=0, tiled=True)  114 us
    all_gather x1, waiting for transfers between devices, on_device(): lax.all_gather(up_weight, 'fs', axis=0, tiled=True)  103 us
    reduce_scatter x1, waiting for transfers between devices, on_device(): lax.psum_scatter(lax.dot_general(block_rows, down_full, (((1,), (1,)), ((...  42.9 us
    all_gather x1, waiting for transfers between devices, on_device(): full_rows = lax.all_gather(hidden_cols, 'tp', axis=1, tiled=True)  32.4 us
    all_gather x1, waiting for transfers between devices, on_device(): lax.all_gather(value_weight, 'fs', axis=0, tiled=True)  25.1 us
    all_gather x1, waiting for transfers between devices, on_device(): lax.all_gather(gate_weight, 'fs', axis=0, tiled=True)  24.4 us
    dot_general x1, matrix products, on_device(): lax.dot_general(block_rows, down_full, (((1,), (1,)), ((), ())), preferre...  23.6 us
  transfers between devices with their start and end apart: 9, of which 8 were waited for; matrix products, arithmetic and copies ran while one was open for 10% of the time, Pallas kernels for 0%

commit v1 on v0

--- a/solution.py
+++ b/solution.py
@@ -79,7 +79,12 @@
         lax.all_gather(up_weight, "fs", axis=0, tiled=True),
         preferred_element_type=jnp.float32,
     )
-    down_full = lax.all_gather(down_weight, "fs", axis=0, tiled=True)
+    ring = [down_weight]
+    for hop in range(3):
+        ring.append(lax.ppermute(ring[-1], "fs", [(dev, (dev + 1) % 4) for dev in range(4)]))
+    down_full = jnp.roll(
+        jnp.concatenate(ring[::-1], axis=0), (lax.axis_index("fs") + 1) * ring[0].shape[0], axis=0
+    )
     product = (jax.nn.silu(causal_conv(ffgate, ff_taps.astype(jnp.float32))) * ff_up).astype(
         jnp.bfloat16
     )

time: 586 us -> 531 us (0.906)
  waiting for transfers between devices: 483 us -> 387 us
  starting transfers between devices: 0.31 us -> 24 us
  local copies, waits for them, and re-layouts: 5.05 us -> 20.8 us
    ppermute x0 -> x3, waiting for transfers between devices: none -> 174 us  [on_device(): lax.ppermute(ring[-1], 'fs', [(dev, (dev + 1) % 4) for dev in range(4)])]
    all_gather x1 -> x0, waiting for transfers between devices: 115 us -> none  [on_device(): down_full = lax.all_gather(down_weight, 'fs', axis=0, tiled=True)]
    all_gather x1, waiting for transfers between devices: 114 us -> 0.02 us  [on_device(): lax.all_gather(ffgate_weight, 'fs', axis=0, tiled=True)]
    all_gather x1, waiting for transfers between devices: 32.4 us -> 0.01 us  [on_device(): full_rows = lax.all_gather(hidden_cols, 'tp', axis=1, tiled=True)]
    ppermute x0 -> x3, starting transfers between devices: none -> 23.7 us  [on_device(): lax.ppermute(ring[-1], 'fs', [(dev, (dev + 1) % 4) for dev in range(4)])]
    unnamed x4 -> x13, local copies, waits for them, and re-layouts: 0.01 us -> 14.5 us
    all_gather x1, waiting for transfers between devices: 103 us -> 95.3 us  [on_device(): lax.all_gather(up_weight, 'fs', axis=0, tiled=True)]
  transfers between devices with their start and end apart: 9 -> 11, of which waited for: 8 -> 8; matrix products, arithmetic and copies ran while one was open for 10% -> 14% of each run, Pallas kernels for 0% -> 0%
where the time goes in v1:
time: 531 us; the launch traced here: 530 us
  waiting for transfers between devices  387 us (73%)
  matrix products  48.8 us (9%)
  other arithmetic  36.1 us (7%)
  starting transfers between devices  24 us (5%)
  local copies, waits for them, and re-layouts  20.8 us (4%)
  between operations  13.7 us (3%)
    ppermute x3, waiting for transfers between devices, on_device(): lax.ppermute(ring[-1], 'fs', [(dev, (dev + 1) % 4) for dev in range(4)])  174 us
    all_gather x1, waiting for transfers between devices, on_device(): lax.all_gather(up_weight, 'fs', axis=0, tiled=True)  95.3 us
    reduce_scatter x1, waiting for transfers between devices, on_device(): lax.psum_scatter(lax.dot_general(block_rows, down_full, (((1,), (1,)), ((...  42.9 us
    all_gather x1, waiting for transfers between devices, on_device(): lax.all_gather(value_weight, 'fs', axis=0, tiled=True)  25.1 us
    all_gather x1, waiting for transfers between devices, on_device(): lax.all_gather(gate_weight, 'fs', axis=0, tiled=True)  24.4 us
    dot_general x1, matrix products, on_device(): lax.dot_general(block_rows, down_full, (((1,), (1,)), ((), ())), preferre...  23.7 us
    ppermute x3, starting transfers between devices, on_device(): lax.ppermute(ring[-1], 'fs', [(dev, (dev + 1) % 4) for dev in range(4)])  23.7 us
    all_gather x1, waiting for transfers between devices, on_device(): lax.all_gather(head_out, 'tp', axis=1, tiled=True)  22.2 us
  transfers between devices with their start and end apart: 11, of which 8 were waited for; matrix products, arithmetic and copies ran while one was open for 14% of the time, Pallas kernels for 0%

profile of v1, /device:TPU:0, one launch (start us, length us, event | category | flops | bytes accessed | tf_op | source)
XLA Modules:
  0.0 530.4 jit_solution(4765043557034046665)
XLA Ops:
  6.5 0.7 all-gather.10.cloned.1.call-update
  7.3 0.7 all-gather.8.cloned.1.call-update
  8.0 0.0 all-gather.14.cloned.1.call-start
  8.1 0.7 all-gather.14.cloned.1.call-update
  8.7 0.0 all-gather.12.cloned.1.call-start
  8.8 1.0 fusion.51
  9.8 1.0 fusion.50
  10.8 0.7 convert_element_type.65
  11.5 3.1 fusion.3
  14.5 0.7 convert_element_type.68
  15.2 24.4 %all-gather.10.cloned.1.call-done = bf16[2048,256]{1,0:T(8,128)(2,1)} async-done(((bf16[512,256]{1,0:T(8,128)(2,1)}), bf16[2048,256]{1,0:T(8,128)(2,1)}) %all-gather.10.cloned.1.call-update) | async-done | bytes 1048592 | tf_op jit(solution)/shard_map/all_gather | solution.py:52
  39.6 3.8 fusion.17
  43.5 25.1 %all-gather.8.cloned.1.call-done = bf16[2048,256]{1,0:T(8,128)(2,1)} async-done(((bf16[512,256]{1,0:T(8,128)(2,1)}), bf16[2048,256]{1,0:T(8,128)(2,1)}) %all-gather.8.cloned.1.call-update) | async-done | bytes 1048592 | tf_op jit(solution)/shard_map/all_gather | solution.py:51
  68.6 3.8 convolution_multiply_fusion
  72.4 4.2 multiply_add_fusion
  76.6 0.5 reshape.42
  77.2 1.1 reduce_sum.37
  78.4 14.4 %multiply_reduce_fusion = f32[1024,2]{1,0:T(8,128)S(1)} fusion(f32[1024,2,128]{2,1,0:T(2,128)S(1)} %reshape.42, f32[1024,2]{1,0:T(8,128)S(1)} %broadcast_multiply_fusion), kind=kLoop, calls=%fused_computation.31 | loop fusion | flops 784384 | bytes 1064960 | tf_op jit(solution)/shard_map/reduce_sum | solution.py:30
  92.8 0.1 add_rsqrt_fusion
  92.9 1.2 mul.524
  94.1 1.2 sub.17
  95.4 5.8 %multiply_convert_fusion.1 = bf16[1024,256]{1,0:T(8,128)(2,1)} fusion(f32[128,8,2,128]{3,2,1,0:T(2,128)S(1)} %bitcast.62, f32[128,8,2,128]{3,2,1,0:T(2,128)S(1)} %bitcast.63, f32[256]{0:T(256)S(1)} %convert_element_type.68, f32[1024,256]{1,0:T(8,128)S(1)} %convolution_multiply_fusion, f32[256]{0:T(256)S(1)} %bitcast.87, f32[256]{0:T(256)S(1)} %bitcast.85, ...), kind=kLoop, calls=%fused_computation.30 | loop fusion | flops 18087936 | bytes 3702784 | tf_op jit(solution)/shard_map/convert_element_type | solution.py:60
  101.2 0.0 all-gather.16.cloned.1.call-start
  101.3 22.2 %all-gather.12.cloned.1.call-done = bf16[1024,1024]{1,0:T(8,128)(2,1)} async-done(((bf16[1024,256]{1,0:T(8,128)(2,1)}), bf16[1024,1024]{1,0:T(8,128)(2,1)}) %all-gather.12.cloned.1.call-update) | async-done | bytes 2097168 | tf_op jit(solution)/shard_map/all_gather | solution.py:63
  123.5 4.4 fusion.14
  127.9 0.0 all-gather.18.cloned.1.call-start
  128.0 0.5 all-gather.18.cloned.1.call-update
  128.6 1.5 collective-permute-start
  130.1 0.0 reduce-scatter.2.cloned.1.call-start
  130.2 36.8 %collective-permute-done = bf16[512,1536]{1,0:T(8,128)(2,1)S(1)} collective-permute-done((bf16[512,1536]{1,0:T(8,128)(2,1)S(1)}, bf16[512,1536]{1,0:T(8,128)(2,1)S(1)}, u32[]{:S(2)}, u32[]{:S(2)}) %collective-permute-start) | collective-permute-done | bytes 1572896 | tf_op jit(solution)/shard_map/ppermute | solution.py:84
  167.0 66.3 %collective-permute-done.1 = bf16[512,1536]{1,0:T(8,128)(2,1)} collective-permute-done((bf16[512,1536]{1,0:T(8,128)(2,1)S(1)}, bf16[512,1536]{1,0:T(8,128)(2,1)}, u32[]{:S(2)}, u32[]{:S(2)}) %collective-permute-start.1) | collective-permute-done | bytes 1572896 | tf_op jit(solution)/shard_map/ppermute | solution.py:84
  233.3 22.2 %collective-permute-start.2 = (bf16[512,1536]{1,0:T(8,128)(2,1)}, bf16[512,1536]{1,0:T(8,128)(2,1)}, u32[]{:S(2)}, u32[]{:S(2)}) collective-permute-start(bf16[512,1536]{1,0:T(8,128)(2,1)} %collective-permute-done.1), channel_id=1, source_target_pairs={{0,4},{4,8},{8,12},{12,0},{1,5},{5,9},{9,13},{13,1},{2,6},{6,10},{... | collective-permute-start | bytes 4718600 | tf_op jit(solution)/shard_map/ppermute | solution.py:84
  255.5 0.1 slice_reduce_fusion.2
  255.5 71.3 %collective-permute-done.2 = bf16[512,1536]{1,0:T(8,128)(2,1)} collective-permute-done((bf16[512,1536]{1,0:T(8,128)(2,1)}, bf16[512,1536]{1,0:T(8,128)(2,1)}, u32[]{:S(2)}, u32[]{:S(2)}) %collective-permute-start.2) | collective-permute-done | bytes 1572896 | tf_op jit(solution)/shard_map/ppermute | solution.py:84
  326.8 2.7 constant_dynamic-update-slice_fusion.7
  329.5 2.7 constant_dynamic-update-slice_fusion.6
  332.1 1.3 constant_dynamic-update-slice_fusion.5
  333.4 1.3 constant_dynamic-update-slice_fusion.4
  334.7 2.7 constant_dynamic-update-slice_fusion.3
  337.3 2.7 constant_dynamic-update-slice_fusion.2
  340.1 1.3 constant_dynamic-update-slice_fusion.1
  341.3 1.3 constant_dynamic-update-slice_fusion
  342.6 3.1 fusion
  345.7 13.0 %fusion.20 = f32[1024,1536]{1,0:T(8,128)} fusion(bf16[2048,1536]{1,0:T(8,128)(2,1)} %all-gather.18.cloned.1.call-done, bf16[1024,2048]{1,0:T(8,128)(2,1)} %all-gather.16.cloned.1.call-done, f32[2048]{0:T(1024)S(1)} %convert_element_type.73, f32[1024]{0:T(1024)S(1)} %add_rsqrt_fusion.1), kind=kOutput, calls=%fused_computation.25 | convolution fusion | flops 6450839552 | bytes 16789504 | tf_op jit(solution)/shard_map/dot_general | solution.py:72
  358.7 95.3 %all-gather.20.cloned.1.call-done = bf16[2048,1536]{1,0:T(8,128)(2,1)} async-done(((bf16[512,1536]{1,0:T(8,128)(2,1)}), bf16[2048,1536]{1,0:T(8,128)(2,1)}) %all-gather.20.cloned.1.call-update) | async-done | bytes 6291472 | tf_op jit(solution)/shard_map/all_gather | solution.py:79
  454.0 23.7 %fusion.8 = bf16[1024,2048]{1,0:T(8,128)(2,1)} fusion(bf16[4096,1536]{1,0:T(8,128)(2,1)} %constant_dynamic-update-slice_fusion, s32[]{:T(128)S(6)} %select_n.22, f32[1024,1536]{1,0:T(8,128)} %fusion.20, bf16[2048,1536]{1,0:T(8,128)(2,1)} %all-gather.20.cloned.1.call-done, f32[1536]{0:T(1024)S(1)} %get-tuple-element.6, f32[1536]{0:T(1024)S(1)} %get-tuple-element.7, ...), kind=kOutput, calls=%fused_computation.13 | convolution fusion | flops 12912689152 | bytes 27293700 | tf_op jit(solution)/shard_map/dot_general | solution.py:94
  477.8 42.9 %reduce-scatter.2.cloned.1.call-done = bf16[256,2048]{1,0:T(8,128)(2,1)} async-done(((bf16[1024,2048]{1,0:T(8,128)(2,1)}), bf16[256,2048]{1,0:T(8,128)(2,1)}) %reduce-scatter.2.cloned.1.call-update) | async-done | bytes 1048592 | tf_op jit(solution)/shard_map/reduce_scatter | solution.py:93
  520.7 2.9 fusion.24
  (22 shorter events, 0.3 us)
Async XLA Ops:
  6.5 33.1 %all-gather.10.cloned.1.call-start = ((), (), s32[]{:S(2)}) async-start(), calls=%async_computation.2 | async-start | bytes 1310720 | tf_op jit(solution)/shard_map/all_gather | solution.py:52
  7.3 61.3 %all-gather.8.cloned.1.call-start = ((), (), s32[]{:S(2)}) async-start(), calls=%async_computation.1 | async-start | bytes 1310720 | tf_op jit(solution)/shard_map/all_gather | solution.py:51
  8.0 93.3 %all-gather.14.cloned.1.call-start = ((), (), s32[]{:S(2)}) async-start(), calls=%async_computation.4 | async-start | bytes 1310720 | tf_op jit(solution)/shard_map/all_gather | solution.py:53
  8.7 114.8 %all-gather.12.cloned.1.call-start = ((), (), s32[]{:S(2)}) async-start(), calls=%async_computation.3 | async-start | bytes 2621440 | tf_op jit(solution)/shard_map/all_gather | solution.py:63
  101.2 241.4 %all-gather.16.cloned.1.call-start = ((), (), s32[]{:S(2)}) async-start(), calls=%async_computation.5 | async-start | bytes 5242880 | tf_op jit(solution)/shard_map/all_gather | solution.py:69
  101.2 27.3 %copy-start = (bf16[512,1536]{1,0:T(8,128)(2,1)S(1)}, bf16[512,1536]{1,0:T(8,128)(2,1)}, u32[]{:S(2)}) copy-start(bf16[512,1536]{1,0:T(8,128)(2,1)} %param.23) | copy-start | bytes 4718596
  101.3 154.2 %copy-start.2 = (bf16[2048]{0:T(1024)(128)(2,1)S(1)}, bf16[2048]{0:T(1024)(128)(2,1)}, u32[]{:S(2)}) copy-start(bf16[2048]{0:T(1024)(128)(2,1)} %param.19) | copy-start | bytes 12292
  101.3 154.2 %copy-start.1 = (bf16[3,1536]{1,0:T(4,128)(2,1)S(1)}, bf16[3,1536]{1,0:T(4,128)(2,1)}, u32[]{:S(2)}) copy-start(bf16[3,1536]{1,0:T(4,128)(2,1)} %param.22) | copy-start | bytes 27652
  127.9 217.8 %all-gather.18.cloned.1.call-start = ((), (), s32[]{:S(2)}) async-start(), calls=%async_computation.6 | async-start | bytes 7864320 | tf_op jit(solution)/shard_map/all_gather | solution.py:74
  128.5 325.5 %all-gather.20.cloned.1.call-start = ((), (), s32[]{:S(2)}) async-start(), calls=%async_computation.7 | async-start | bytes 7864320 | tf_op jit(solution)/shard_map/all_gather | solution.py:79
  128.6 38.4 %collective-permute-start = (bf16[512,1536]{1,0:T(8,128)(2,1)S(1)}, bf16[512,1536]{1,0:T(8,128)(2,1)S(1)}, u32[]{:S(2)}, u32[]{:S(2)}) collective-permute-start(bf16[512,1536]{1,0:T(8,128)(2,1)S(1)} %copy-done), channel_id=1, source_target_pairs={{0,4},{4,8},{8,12},{12,0},{1,5},{5,9},{9,13},{13,1},{2,6},{6,10},{... | collective-permute-start | bytes 4718600 | tf_op jit(solution)/shard_map/ppermute | solution.py:84
  130.1 390.5 %reduce-scatter.2.cloned.1.call-start = ((), (), s32[]{:S(2)}) async-start(), calls=%async_computation.8 | async-start | bytes 5242880 | tf_op jit(solution)/shard_map/reduce_scatter | solution.py:93
  167.0 66.3 %collective-permute-start.1 = (bf16[512,1536]{1,0:T(8,128)(2,1)S(1)}, bf16[512,1536]{1,0:T(8,128)(2,1)}, u32[]{:S(2)}, u32[]{:S(2)}) collective-permute-start(bf16[512,1536]{1,0:T(8,128)(2,1)S(1)} %collective-permute-done), channel_id=1, source_target_pairs={{0,4},{4,8},{8,12},{12,0},{1,5},{5,9},{9,13},{13,1},{2,6},{6,10},{... | collective-permute-start | bytes 4718600 | tf_op jit(solution)/shard_map/ppermute | solution.py:84
  233.3 93.6 %collective-permute-start.2 = (bf16[512,1536]{1,0:T(8,128)(2,1)}, bf16[512,1536]{1,0:T(8,128)(2,1)}, u32[]{:S(2)}, u32[]{:S(2)}) collective-permute-start(bf16[512,1536]{1,0:T(8,128)(2,1)} %collective-permute-done.1), channel_id=1, source_target_pairs={{0,4},{4,8},{8,12},{12,0},{1,5},{5,9},{9,13},{13,1},{2,6},{6,10},{... | collective-permute-start | bytes 4718600 | tf_op jit(solution)/shard_map/ppermute | solution.py:84
Sparse Core Ops, SparseCore 0:
  8.9 30.6 all-gather.9
  41.2 27.3 all-gather.7
  70.2 27.3 all-gather.13
  101.3 22.1 all-gather.11
  128.1 34.4 all-gather.15
  164.0 175.7 all-gather.17
  341.4 112.5 all-gather.19
  477.9 42.7 reduce-scatter.1
